TPU v7x, 256 devices: a whole 4x4x8 slice. The times are simulated.
256 devices in a mesh: ep: 16 (over y, x), tp: 16 (over z, core).
Axes of the slice: x: 4, y: 4, z: 8, core: 2. Of those that a mesh axis runs over, the one named last changes fastest.
Arguments:
- tokens: bfloat16 [16384, 2048], P('ep', 'tp'), may hold values from -48 to 48
- pre_gain: bfloat16 [2048], P('tp'), may hold values from 0.099609375 to 1.8984375
- route_ids: int32 [16384, 2], P('ep'), may hold values from 0 to 15, all different within a row; in each aligned block of 1024 rows (0 to 1023, 1024 to 2047, ...) at most 144 rows name the same one
- route_weights: float32 [16384, 2], P('ep'), may hold values from 0.1 to 1
- gate_weight: bfloat16 [16, 2048, 7168], P('ep', None, 'tp'), may hold values from -0.125 to 0.125
- up_weight: bfloat16 [16, 2048, 7168], P('ep', None, 'tp'), may hold values from -0.125 to 0.125
- down_weight: bfloat16 [16, 7168, 2048], P('ep', 'tp')
- post_gain: bfloat16 [2048], P('tp'), may hold values from 0.099609375 to 1.8984375
Outputs:
- mixed: bfloat16 [16384, 2048], P('ep', 'tp')
Inputs may be any that keep to these rules, and one draw needn't show every extreme that they name: `route_ids`: each row names 2 different experts; among the rows of one index of ep no expert is named more than 144 times, a bound that some block reaches.
All inputs are finite; a program needn't handle non-finite values.
Results may differ from a plain program's by a relative error of at most 0.02.
Values may be sent and summed in bfloat16 or wider, within the bound.
A program may use at most 128 MiB of HBM per device.

v0:
```python
import jax
import jax.numpy as jnp
from jax import lax
from jax.sharding import PartitionSpec as P

D = 2048


epsilon = 1e-06


def copy_for_each(value, axis):
    count = lax.axis_size(axis)
    return lax.all_to_all(
        jnp.broadcast_to(value[None], (count, *value.shape)), axis, 0, 0, tiled=True
    )


def of_everyone(value, axis):
    everything = copy_for_each(value, axis)
    return jnp.sum(everything, axis=0)


def run_expert(routed, gate_weight, up_weight, down_weight):
    gate_block = gate_weight[0]
    up_block = up_weight[0]
    down_block = down_weight[0]
    piece = lax.all_gather(routed, "tp", axis=1, tiled=True)
    gate_act = jnp.dot(piece, gate_block, preferred_element_type=jnp.float32)
    up_act = jnp.dot(piece, up_block, preferred_element_type=jnp.float32)
    hidden = (jax.nn.silu(gate_act) * up_act).astype(jnp.bfloat16)
    partial_value = jnp.dot(hidden, down_block, preferred_element_type=jnp.float32)
    return lax.psum_scatter(
        partial_value.astype(jnp.bfloat16), "tp", scatter_dimension=1, tiled=True
    )


def on_device(
    tokens, pre_gain, route_ids, route_weights, gate_weight, up_weight, down_weight, post_gain
):
    tok_rows, columns = tokens.shape
    top_count = route_ids.shape[1]
    groups = lax.axis_size("ep")
    capacity = 9 * tok_rows * top_count // (8 * groups)
    values = tokens.astype(jnp.float32)
    squares = of_everyone(jnp.sum(values * values, axis=1), "tp")
    normed = (
        values * lax.rsqrt(squares / D + epsilon)[:, None] * pre_gain.astype(jnp.float32)[None, :]
    ).astype(jnp.bfloat16)
    flat_ids = route_ids.reshape(-1)
    onehot = (flat_ids[:, None] == jnp.arange(groups, dtype=jnp.int32)[None, :]).astype(jnp.int32)
    slot_rank = jnp.sum((jnp.cumsum(onehot, axis=0) - 1) * onehot, axis=1)
    positions = jnp.arange(tok_rows * top_count, dtype=jnp.int32)
    slot_table = (
        jnp.full((groups, capacity), tok_rows * top_count, jnp.int32)
        .at[flat_ids, slot_rank]
        .set(positions)
    )
    padded = jnp.concatenate([normed, jnp.zeros((1, columns), jnp.bfloat16)], axis=0)
    outgoing = padded[slot_table // top_count]
    arrived = lax.all_to_all(outgoing, "ep", split_axis=0, concat_axis=0, tiled=True)
    results = run_expert(arrived.reshape(-1, columns), gate_weight, up_weight, down_weight)
    returned = lax.all_to_all(
        results.reshape(groups, capacity, columns), "ep", split_axis=0, concat_axis=0, tiled=True
    )
    copies = returned.reshape(-1, columns)[flat_ids * capacity + slot_rank]
    copies = copies.astype(jnp.float32).reshape(tok_rows, top_count, columns)
    combined = jnp.sum(copies * route_weights[:, :, None], axis=1)
    totals = of_everyone(jnp.sum(combined * combined, axis=1), "tp")
    scaled = combined * lax.rsqrt(totals / D + epsilon)[:, None]
    return (scaled * post_gain.astype(jnp.float32)[None, :]).astype(jnp.bfloat16)


def solution(mesh):
    placed = (
        P("ep", "tp"),
        P("tp"),
        P("ep", None),
        P("ep", None),
        P("ep", None, "tp"),
        P("ep", None, "tp"),
        P("ep", "tp", None),
        P("tp"),
    )
    return jax.shard_map(
        on_device, mesh=mesh, in_specs=placed, out_specs=P("ep", "tp"), check_vma=False
    )
```

profile of v0, /device:TPU:1, one launch (start us, length us, event | category | flops | bytes accessed | tf_op | source)
XLA Modules:
  0.0 292.6 jit_solution(6376874035539281502)
XLA Ops:
  6.5 1.3 fusion.7
  7.8 0.7 broadcast_in_dim.8
  8.5 10.0 %all-to-all-start = ((f32[16,1,1024]{2,1,0:T(1,128)}), f32[16,1,1024]{2,1,0:T(1,128)S(1)}, u32[]{:S(2)}, u32[]{:S(2)}) async-start(f32[16,1,1024]{2,1,0:T(1,128)} %broadcast_in_dim.8), calls=%async_computation | async-start | bytes 131072 | tf_op jit(solution)/shard_map/all_to_all | solution.py:14
  18.5 0.9 copy.23
  20.3 4.5 %reduce-window.6 = s32[16,16,128]{2,1,0:T(8,128)S(1)} reduce-window(s32[16,16,128]{2,1,0:T(8,128)S(1)} %fusion.12, s32[]{:T(128)} %constant.38.clone.1), window={size=1x1x128 pad=0_0x0_0x127_0}, to_apply=%region_2.0 | reduce-window | flops 4161536 | bytes 262148 | tf_op jit(solution)/shard_map/reduce-window
  25.7 0.7 multiply_reduce_fusion.1
  26.4 0.8 and_reduce_fusion
  27.2 8.1 %scatter_custom_fusion = s32[2304]{0:T(1024)S(1)} fusion(s32[2048]{0:T(1024)S(1)} %broadcast_select_fusion, s32[2048]{0:T(1024)S(1)} %iota.11, s32[]{:T(128)} %constant.37.clone.1), kind=kCustom, calls=%fused_computation.42 | custom fusion | bytes 9220
  36.2 1.2 fusion.9
  37.4 4.7 %gather_fusion = bf16[2304,128]{1,0:T(8,128)(2,1)S(1)} fusion(bf16[1025,128]{1,0:T(8,128)(2,1)S(1)} %concatenate.6, s32[3072]{0:T(1024)S(1)} %pad_clamp_fusion), kind=kCustom, calls=%fused_computation | custom fusion | bytes 1188864 | tf_op jit(solution)/shard_map/gather | solution.py:60
  42.1 18.3 %all_to_all.22 = bf16[16,144,128]{2,1,0:T(8,128)(2,1)} all-to-all(bf16[16,144,128]{2,1,0:T(8,128)(2,1)S(1)} %bitcast.39), channel_id=1, replica_groups=mesh['ep'=16,'tp'=16] {'ep'}, dimensions={0} | all-to-all | bytes 1179648 | tf_op jit(solution)/shard_map/all_to_all | solution.py:61
  60.7 68.6 %all-gather.2.cloned.1.call-done = bf16[2304,2048]{1,0:T(8,128)(2,1)} async-done(((bf16[2304,128]{1,0:T(8,128)(2,1)}), bf16[2304,2048]{1,0:T(8,128)(2,1)}) %all-gather.2.cloned.1.call-update) | async-done | bytes 9437200 | tf_op jit(solution)/shard_map/all_gather | solution.py:28
  129.3 10.7 %fusion.4 = f32[2304,448]{0,1:T(8,128)} fusion(bf16[2304,2048]{1,0:T(8,128)(2,1)} %all-gather.2.cloned.1.call-done, bf16[1,2048,448]{1,2,0:T(8,128)(2,1)} %param.12), kind=kOutput, calls=%fused_computation.8 | convolution fusion | flops 4227858432 | bytes 15400960 | tf_op jit(solution)/shard_map/dot_general | solution.py:29
  139.9 17.7 %convolution_convert_fusion = bf16[2304,2048]{1,0:T(8,128)(2,1)} fusion(bf16[1,448,2048]{2,1,0:T(8,128)(2,1)S(1)} %copy-done, bf16[2304,2048]{1,0:T(8,128)(2,1)} %all-gather.2.cloned.1.call-done, f32[2304,448]{0,1:T(8,128)} %fusion.4, bf16[1,2048,448]{1,2,0:T(8,128)(2,1)} %param.13), kind=kOutput, calls=%fused_computation.3 | convolution fusion | flops 8466628608 | bytes 26673152 | tf_op jit(solution)/shard_map/dot_general | solution.py:32
  157.7 12.2 %copy.28 = bf16[2304,2048]{0,1:T(8,128)(2,1)} copy(bf16[2304,2048]{1,0:T(8,128)(2,1)} %convolution_convert_fusion) | data formatting | bytes 18874368
  169.8 66.5 %reduce-scatter.4.cloned.1.call-done = bf16[128,2304]{1,0:T(8,128)(2,1)} async-done(((bf16[2048,2304]{1,0:T(8,128)(2,1)}), bf16[128,2304]{1,0:T(8,128)(2,1)}) %reduce-scatter.4.cloned.1.call-update) | async-done | bytes 589840
  236.3 2.1 copy.29
  238.4 6.8 %all-to-all-start.2 = ((bf16[16,144,128]{2,1,0:T(8,128)(2,1)}), bf16[16,144,128]{2,1,0:T(8,128)(2,1)S(1)}, u32[]{:S(2)}, u32[]{:S(2)}) async-start(bf16[16,144,128]{2,1,0:T(8,128)(2,1)} %bitcast.7), calls=%async_computation.2 | async-start | bytes 1179648 | tf_op jit(solution)/shard_map/all_to_all | solution.py:63
  245.4 9.1 %all-to-all-done.2 = bf16[16,144,128]{2,1,0:T(8,128)(2,1)S(1)} async-done(((bf16[16,144,128]{2,1,0:T(8,128)(2,1)}), bf16[16,144,128]{2,1,0:T(8,128)(2,1)S(1)}, u32[]{:S(2)}, u32[]{:S(2)}) %all-to-all-start.2) | async-done | bytes 589856 | tf_op jit(solution)/shard_map/all_to_all | solution.py:63
  254.5 6.2 %gather_fusion.1 = bf16[2048,128]{1,0:T(8,128)(2,1)S(1)} fusion(bf16[2304,128]{1,0:T(8,128)(2,1)S(1)} %bitcast.36, s32[2048]{0:T(1024)S(1)} %broadcast_clamp_fusion), kind=kCustom, calls=%fused_computation.1 | custom fusion | bytes 1056768 | tf_op jit(solution)/shard_map/gather | solution.py:66
  260.7 5.6 %fusion.6 = f32[1024,128]{1,0:T(8,128)S(1)} fusion(bf16[1024,2,128]{2,1,0:T(2,128)(2,1)S(1)} %bitcast.40, f32[1024,2]{1,0:T(8,128)S(1)} %copy.26), kind=kLoop, calls=%fused_computation.11 | loop fusion | flops 655360 | bytes 1056768 | tf_op jit(solution)/shard_map/reduce_sum | solution.py:68
  267.2 9.8 %all-to-all-start.3 = ((f32[16,1,1024]{2,1,0:T(1,128)}), f32[16,1,1024]{2,1,0:T(1,128)S(1)}, u32[]{:S(2)}, u32[]{:S(2)}) async-start(f32[16,1,1024]{2,1,0:T(1,128)} %broadcast_in_dim.11), calls=%async_computation.3 | async-start | bytes 131072 | tf_op jit(solution)/shard_map/all_to_all | solution.py:14
  277.1 7.8 %all-to-all-done.3 = f32[16,1,1024]{2,1,0:T(1,128)S(1)} async-done(((f32[16,1,1024]{2,1,0:T(1,128)}), f32[16,1,1024]{2,1,0:T(1,128)S(1)}, u32[]{:S(2)}, u32[]{:S(2)}) %all-to-all-start.3) | async-done | bytes 65568 | tf_op jit(solution)/shard_map/all_to_all | solution.py:14
  284.9 0.9 multiply_convert_fusion
  (37 shorter events, 4.1 us)
Async XLA Ops:
  6.5 133.4 %copy-start = (bf16[1,448,2048]{2,1,0:T(8,128)(2,1)S(1)}, bf16[1,448,2048]{2,1,0:T(8,128)(2,1)}, u32[]{:S(2)}) copy-start(bf16[1,448,2048]{2,1,0:T(8,128)(2,1)} %param.14) | copy-start | bytes 5505028
  8.5 27.7 %all-to-all-start = ((f32[16,1,1024]{2,1,0:T(1,128)}), f32[16,1,1024]{2,1,0:T(1,128)S(1)}, u32[]{:S(2)}, u32[]{:S(2)}) async-start(f32[16,1,1024]{2,1,0:T(1,128)} %broadcast_in_dim.8), calls=%async_computation | async-start | bytes 131072 | tf_op jit(solution)/shard_map/all_to_all | solution.py:14
  18.5 110.8 %all-gather.2.cloned.1.call-start = ((), (), s32[]{:S(2)}) async-start(), calls=%async_computation.5 | async-start | bytes 10027008 | tf_op jit(solution)/shard_map/all_gather | solution.py:28
  60.4 175.9 %reduce-scatter.4.cloned.1.call-start = ((), (), s32[]{:S(2)}) async-start(), calls=%async_computation.6 | async-start | bytes 10027008
  169.8 75.4 %copy-start.1 = (f32[1024,2]{0,1:T(2,128)S(1)}, f32[1024,2]{0,1:T(2,128)}, u32[]{:S(2)}) copy-start(f32[1024,2]{0,1:T(2,128)} %param.11) | copy-start | bytes 24580
  238.4 38.6 %copy-start.2 = (bf16[128]{0:T(256)(128)(2,1)S(1)}, bf16[128]{0:T(256)(128)(2,1)}, u32[]{:S(2)}) copy-start(bf16[128]{0:T(256)(128)(2,1)} %param.15) | copy-start | bytes 772
  238.4 16.1 %all-to-all-start.2 = ((bf16[16,144,128]{2,1,0:T(8,128)(2,1)}), bf16[16,144,128]{2,1,0:T(8,128)(2,1)S(1)}, u32[]{:S(2)}, u32[]{:S(2)}) async-start(bf16[16,144,128]{2,1,0:T(8,128)(2,1)} %bitcast.7), calls=%async_computation.2 | async-start | bytes 1179648 | tf_op jit(solution)/shard_map/all_to_all | solution.py:63
  267.2 17.6 %all-to-all-start.3 = ((f32[16,1,1024]{2,1,0:T(1,128)}), f32[16,1,1024]{2,1,0:T(1,128)S(1)}, u32[]{:S(2)}, u32[]{:S(2)}) async-start(f32[16,1,1024]{2,1,0:T(1,128)} %broadcast_in_dim.11), calls=%async_computation.3 | async-start | bytes 131072 | tf_op jit(solution)/shard_map/all_to_all | solution.py:14
Sparse Core Ops, SparseCore 0:
  60.6 68.6 all-gather.1
  170.0 66.2 reduce-scatter.3
where the time goes:
time: 293 us
  waiting for transfers between devices  152 us (52%)
  local copies, waits for them, and re-layouts  37.1 us (13%)
  matrix products  28.4 us (10%)
  starting transfers between devices  26.8 us (9%)
  blocking collectives  18.3 us (6%)
  other arithmetic  16.4 us (6%)
  between operations  13.6 us (5%)
    all_gather x1, waiting for transfers between devices, run_expert(): piece = lax.all_gather(routed, 'tp', axis=1, tiled=True)  68.6 us
    unnamed x3, waiting for transfers between devices  66.5 us
    unnamed x11, local copies, waits for them, and re-layouts  23.5 us
    all_to_all x2, starting transfers between devices, copy_for_each(): lax.all_to_all(jnp.broadcast_to(value[None], (count, *value.shape)), axis...  19.8 us
    all_to_all x1, blocking collectives, on_device(): lax.all_to_all(outgoing, 'ep', split_axis=0, concat_axis=0, tiled=True)  18.3 us
    dot_general x1, matrix products, run_expert(): jnp.dot(hidden, down_block, preferred_element_type=jnp.float32)  17.7 us
    dot_general x1, matrix products, run_expert(): gate_act = jnp.dot(piece, gate_block, preferred_element_type=jnp.float32)  10.7 us
    all_to_all x1, waiting for transfers between devices, on_device(): lax.all_to_all(results.reshape(groups, capacity, columns), 'ep', split_ax...  9.08 us
  transfers between devices with their start and end apart: 5, of which 4 were waited for; matrix products, arithmetic and copies ran while one was open for 6% of the time, Pallas kernels for 0%

commit v1 on v0

v1 whole, which is shorter than its diff:
```python
import functools

import jax
import jax.numpy as jnp
from jax import lax
from jax.experimental import pallas as pl
from jax.experimental.pallas import tpu as pltpu
from jax.sharding import PartitionSpec as P

BF, F32 = jnp.bfloat16, jnp.float32
MESH = pl.DeviceIdType.MESH
NX = 4
EPS = 1e-06
LANES = 128
NT = (((1,), (1,)), ((), ()))


def near_first(i, n):
    return i if n < 4 else i + lax.div(i, 2) - 2 * lax.div(i, 3)


def kernel(
    dims,
    tokens, ids, weights, pre_gain, post_gain, gate_hbm, up_hbm, down_hbm,
    out,
    gates, downs, ranks, cols, outgoing, gains, x_all, x_norm, hidden,
    part, peer_part, ring_out, ring_in, results, returned, sums, squares, square_own,
    w_sem, gain_s, gain_r, disp_s, disp_r, ag_s, ag_r, d2d_s, d2d_r,
    pp_s, pp_r, rs_s, rs_r, ret_s, ret_r, sq_s, sq_r,
):
    ny, nx, nz, cap, per_chunk, width = dims
    n_ep, n_tp = ny * nx, nz * 2
    chunks = n_ep // per_chunk
    rows = cap * per_chunk
    half = rows // 2
    hops = nz // 2
    toks = tokens.shape[0]
    hid = gate_hbm.shape[0]
    hid_pad = downs.shape[0]

    ep, tp = lax.axis_index("ep"), lax.axis_index("tp")
    y, x = lax.div(ep, nx), lax.rem(ep, nx)
    z, core = lax.div(tp, 2), lax.rem(tp, 2)
    peer = z * 2 + 1 - core
    right = lax.rem(z + 1, nz) * 2 + core
    left = lax.rem(z + nz - 1, nz) * 2 + core

    def remote(src, dst, ssem, rsem, ep_to, tp_to):
        return pltpu.make_async_remote_copy(
            src_ref=src, dst_ref=dst, send_sem=ssem, recv_sem=rsem,
            device_id=(ep_to, tp_to), device_id_type=MESH,
        )

    barrier = pltpu.get_barrier_semaphore()

    def greet_ep(i, _):
        pl.semaphore_signal(barrier, inc=1, device_id=(lax.rem(ep + i, n_ep), tp), device_id_type=MESH)
        return 0

    def greet_tp(i, _):
        pl.semaphore_signal(barrier, inc=1, device_id=(ep, lax.rem(tp + i, n_tp)), device_id_type=MESH)
        return 0

    lax.fori_loop(1, n_ep, greet_ep, 0)
    lax.fori_loop(1, n_tp, greet_tp, 0)

    loads = (
        pltpu.make_async_copy(gate_hbm, gates.at[pl.ds(0, hid)], w_sem.at[0]),
        pltpu.make_async_copy(up_hbm, gates.at[pl.ds(hid_pad, hid)], w_sem.at[1]),
        pltpu.make_async_copy(down_hbm, downs.at[pl.ds(0, hid)], w_sem.at[2]),
    )
    for load in loads:
        load.start()
    if hid_pad > hid:
        gates[pl.ds(hid, hid_pad - hid), :] = jnp.zeros((hid_pad - hid, width), BF)
        gates[pl.ds(hid_pad + hid, hid_pad - hid), :] = jnp.zeros((hid_pad - hid, width), BF)
        downs[pl.ds(hid, hid_pad - hid), :] = jnp.zeros((hid_pad - hid, width), BF)
    gains[tp] = jnp.broadcast_to(pre_gain[...].astype(F32), (8, LANES))

    o_i = lax.broadcasted_iota(jnp.int32, (n_ep, toks), 0)
    a_i, b_i = o_i // nx, o_i % nx

    def near_vec(i, n):
        return i if n < 4 else jnp.where(i == 2, 3, jnp.where(i == 3, 2, i))

    e_of = ((y + near_vec(a_i, ny)) % ny) * nx + (x + near_vec(b_i, nx)) % nx
    first = (ids[0:1, :] == e_of).astype(F32)
    second = (ids[1:2, :] == e_of).astype(F32)
    named = first + second
    named_bf = named.astype(BF)
    step = min(256, toks)
    for at in range(0, toks, step):
        before = lax.broadcasted_iota(jnp.int32, (toks, step), 0)
        after = lax.broadcasted_iota(jnp.int32, (toks, step), 1) + at
        upper = jnp.where(before < after, 1.0, 0.0).astype(BF)
        ranks[:, pl.ds(at, step)] = jnp.dot(named_bf, upper, preferred_element_type=F32)
    rank = ranks[...]
    slot = o_i.astype(F32) * float(cap) + rank
    slot0 = jnp.sum(first * slot, axis=0, keepdims=True)
    slot1 = jnp.sum(second * slot, axis=0, keepdims=True)
    ranks[...] = jnp.where(named > 0.0, rank, -1.0)
    r8 = lax.broadcasted_iota(jnp.int32, (8, toks), 0)
    table = jnp.where(r8 == 0, slot0, jnp.where(r8 == 1, slot1, jnp.where(r8 == 2, weights[0:1, :], weights[1:2, :])))
    cols[...] = table.T

    pl.semaphore_wait(barrier, n_ep - 1 + n_tp - 1)

    def send_gain(i, _):
        remote(gains.at[tp], gains.at[tp], gain_s.at[i], gain_r.at[i], ep, lax.rem(tp + i, n_tp)).start()
        return 0

    lax.fori_loop(1, n_tp, send_gain, 0)

    def block_peer(o, sign):
        dy = near_first(lax.div(o, nx), ny)
        dx = near_first(lax.rem(o, nx), nx)
        return lax.rem(y + ny + sign * dy, ny) * nx + lax.rem(x + nx + sign * dx, nx)

    def block_rows(o):
        return pl.ds(pl.multiple_of(o * cap, 16), cap)

    def dispatch_copy(o):
        return remote(
            outgoing.at[o], x_all.at[tp, block_rows(o)], disp_s.at[o], disp_r.at[o], block_peer(o, 1), tp
        )

    s_i = lax.broadcasted_iota(jnp.int32, (cap, toks), 0).astype(F32)

    def dispatch(o, _):
        pick = jnp.where(s_i == ranks[pl.ds(o, 1), :], 1.0, 0.0).astype(BF)
        picked = jnp.dot(pick, tokens[...], preferred_element_type=F32).astype(BF)

        @pl.when(o == 0)
        def _():
            x_all[tp, pl.ds(0, cap)] = picked

        @pl.when(o > 0)
        def _():
            outgoing[o] = picked
            dispatch_copy(o).start()

        return 0

    lax.fori_loop(0, n_ep, dispatch, 0)

    def chunk_rows(c, at=0, count=None):
        return pl.ds(pl.multiple_of(c * rows + at, 16), rows if count is None else count)

    def slice_at(h):
        return lax.rem(z + 2 * nz - h, nz) * 2 + core

    def ag_copy(c, h, way):
        j = slice_at(h - 1 if way == 0 else 1 - h)
        at, count = (0, rows) if h < hops else ((0, half) if way == 0 else (half, half))
        ref = x_all.at[j, chunk_rows(c, at, count)]
        return remote(ref, ref, ag_s.at[c, way, h - 1], ag_r.at[c, way, h - 1], ep, right if way == 0 else left)

    def ag_arrived(c, h, way):
        j = slice_at(h if way == 0 else -h)
        at, count = (0, rows) if h < hops else ((0, half) if way == 0 else (half, half))
        ref = x_all.at[j, chunk_rows(c, at, count)]
        remote(ref, ref, ag_s.at[c, way, h - 1], ag_r.at[c, way, h - 1], ep, right).wait_recv()

    def d2d_copy(c, q):
        ref = x_all.at[slice_at(q), chunk_rows(c)]
        return remote(ref, ref, d2d_s.at[c, lax.rem(q + nz, nz)], d2d_r.at[c, lax.rem(q + nz, nz)], ep, peer)

    def d2d_arrived(c, q):
        j = lax.rem(z + 2 * nz - q, nz) * 2 + 1 - core
        ref = x_all.at[j, chunk_rows(c)]
        remote(ref, ref, d2d_s.at[c, q], d2d_r.at[c, q], ep, peer).wait_recv()

    def gather_first(c):
        for b in range(per_chunk):
            o = c * per_chunk + b

            @pl.when(o > 0)
            def _():
                dispatch_copy(o).wait_recv()

        ag_copy(c, 1, 0).start()
        ag_copy(c, 1, 1).start()
        d2d_copy(c, 0).start()

    def gather_hop(c, h):
        for way in (0, 1):
            ag_arrived(c, h, way)
            if h < hops:
                ag_copy(c, h + 1, way).start()
                d2d_copy(c, h if way == 0 else -h).start()
        if h == hops:
            d2d_copy(c, h).start()

    def feed_forward(c):
        @pl.when(c == 0)
        def _():
            for load in loads:
                load.wait()

            def gain_arrived(i, _):
                remote(gains.at[tp], gains.at[tp], gain_s.at[i], gain_r.at[i], ep, tp).wait_recv()
                return 0

            lax.fori_loop(1, n_tp, gain_arrived, 0)

        for q in range(nz):
            d2d_arrived(c, q)

        def norm(i, _):
            at = pl.ds(pl.multiple_of(c * rows + i * 16, 16), 16)
            vals = [x_all[j, at].astype(F32) for j in range(n_tp)]
            total = vals[0] * vals[0]
            for v in vals[1:]:
                total = total + v * v
            scale = lax.rsqrt(jnp.sum(total, axis=1, keepdims=True) / width + EPS)
            to = pl.ds(pl.multiple_of(i * 16, 16), 16)
            for j, v in enumerate(vals):
                x_norm[to, j * LANES:(j + 1) * LANES] = (v * scale * gains[j, 0:1, :]).astype(BF)
            return 0

        lax.fori_loop(0, rows // 16, norm, 0)
        tile = min(256, hid_pad)
        for at in range(0, hid_pad, tile):
            g = lax.dot_general(x_norm[...], gates[at:at + tile, :], NT, preferred_element_type=F32)
            u = lax.dot_general(x_norm[...], gates[hid_pad + at:hid_pad + at + tile, :], NT, preferred_element_type=F32)
            hidden[:, at:at + tile] = (g / (1.0 + jnp.exp(-g)) * u).astype(BF)

        for m in range(nz):
            p = jnp.dot(hidden[...], downs[:, m * 256:(m + 1) * 256], preferred_element_type=F32).astype(BF)
            part[c, 0, m] = p[:, :LANES]
            part[c, 1, m] = p[:, LANES:]
        peer_copy(c).start()

    def peer_copy(c):
        return remote(part.at[c, 1 - core], peer_part.at[c], pp_s.at[c], pp_r.at[c], ep, peer)

    def chip_sum(c, zd, at=0, count=None):
        sl = pl.ds(at, rows if count is None else count)
        return part[c, core, zd, sl, :].astype(F32) + peer_part[c, zd, sl, :].astype(F32)

    def rs_copy(c, s, way):
        at, count = (0, rows) if s > 1 else ((0, half) if way == 0 else (half, half))
        sl = pl.ds(at, count)
        return remote(
            ring_out.at[c, way, s - 1, sl], ring_in.at[c, way, s - 1, sl],
            rs_s.at[c, way, s - 1], rs_r.at[c, way, s - 1], ep, right if way == 0 else left,
        )

    def scatter_stage(c, s):
        if s == 1:
            peer_copy(c).wait_recv()
        for way in (0, 1):
            far = hops + 1 - s
            zd = lax.rem(z + far, nz) if way == 0 else lax.rem(z + nz - far, nz)
            if s == 1:
                at = 0 if way == 0 else half
                ring_out[c, way, 0, at:at + half, :] = chip_sum(c, zd, at, half).astype(BF)
            else:
                rs_copy(c, s - 1, way).wait_recv()
                for at in (0, half):
                    v = chip_sum(c, zd, at, half)
                    if s > 2 or (at == 0) == (way == 0):
                        v = v + ring_in[c, way, s - 2, at:at + half, :].astype(F32)
                    ring_out[c, way, s - 1, at:at + half, :] = v.astype(BF)
            rs_copy(c, s, way).start()

    def return_copy(o):
        return remote(
            results.at[block_rows(o)], returned.at[block_rows(o)], ret_s.at[o], ret_r.at[o], block_peer(o, -1), tp
        )

    def finish(c):
        for way in (0, 1):
            rs_copy(c, hops, way).wait_recv()
        for b in range(per_chunk):
            o = c * per_chunk + b
            at = b * cap
            v = chip_sum(c, z, at, cap)
            if hops > 1 or b * cap < half:
                v = v + ring_in[c, 0, hops - 1, at:at + cap, :].astype(F32)
            if hops > 1 or b * cap >= half:
                v = v + ring_in[c, 1, hops - 1, at:at + cap, :].astype(F32)
            v = v.astype(BF)

            @pl.when(o == 0)
            def _():
                returned[pl.ds(0, cap), :] = v

            @pl.when(o > 0)
            def _():
                results[block_rows(o), :] = v
                return_copy(o).start()

    def combine(c):
        for b in range(per_chunk):
            o = c * per_chunk + b

            @pl.when(o > 0)
            def _():
                return_copy(o).wait_recv()

        lane = lax.broadcasted_iota(jnp.int32, (toks, rows), 1).astype(F32) + (c * rows).astype(F32)
        values = returned[chunk_rows(c), :]
        for k in (0, 1):
            pick = jnp.where(lane == cols[:, k:k + 1], 1.0, 0.0).astype(BF)
            got = jnp.dot(pick, values, preferred_element_type=F32)

            @pl.when(c == 0)
            def _():
                sums[k] = got

            @pl.when(c > 0)
            def _():
                sums[k] = sums[k] + got

    stages = [gather_first]
    stages += [functools.partial(gather_hop, h=h) for h in range(1, hops + 1)]
    stages += [feed_forward]
    stages += [functools.partial(scatter_stage, s=s) for s in range(1, hops + 1)]
    stages += [finish, combine]

    def slot_step(t, _):
        for k, stage in enumerate(stages):
            c = t - k

            @pl.when((c >= 0) & (c < chunks))
            def _():
                stage(c)

        return 0

    lax.fori_loop(0, chunks + len(stages) - 1, slot_step, 0)

    both = cols[:, 2:3] * sums[0] + cols[:, 3:4] * sums[1]
    sums[0] = both
    square_own[...] = jnp.sum((both * both).T, axis=0, keepdims=True)

    def square_copy(i):
        return remote(square_own, squares.at[i], sq_s.at[i], sq_r.at[i], ep, lax.rem(tp + i, n_tp))

    def send_square(i, _):
        square_copy(i).start()
        return 0

    lax.fori_loop(1, n_tp, send_square, 0)

    def drain_block(o, _):
        dispatch_copy(o).wait_send()
        return_copy(o).wait_send()
        return 0

    lax.fori_loop(1, n_ep, drain_block, 0)

    def drain_chunk(c, _):
        for h in range(1, hops + 1):
            for way in (0, 1):
                ag_copy(c, h, way).wait_send()
                rs_copy(c, h, way).wait_send()
        for q in range(nz):
            d2d_copy(c, q).wait_send()
        peer_copy(c).wait_send()
        return 0

    lax.fori_loop(0, chunks, drain_chunk, 0)

    def drain_gain(i, _):
        remote(gains.at[tp], gains.at[tp], gain_s.at[i], gain_r.at[i], ep, tp).wait_send()
        return 0

    lax.fori_loop(1, n_tp, drain_gain, 0)

    total = square_own[...]
    for i in range(1, n_tp):
        square_copy(i).wait_recv()
        total = total + squares[i]
    scale = lax.rsqrt(total / width + EPS)
    scale = jnp.broadcast_to(scale, (8, toks)).T
    out[...] = (sums[0] * scale[:, 0:1] * post_gain[...].astype(F32)).astype(BF)

    def drain_square(i, _):
        square_copy(i).wait_send()
        return 0

    lax.fori_loop(1, n_tp, drain_square, 0)


def make(dims, toks, hid):
    ny, nx, nz, cap, per_chunk, width = dims
    n_ep, n_tp = ny * nx, nz * 2
    chunks, rows, hops = n_ep // per_chunk, cap * per_chunk, nz // 2
    hid_pad = -(-hid // 256) * 256 if hid > 128 else 128
    vmem = pl.BlockSpec(memory_space=pltpu.VMEM)
    hbm = pl.BlockSpec(memory_space=pl.ANY)
    dma = pltpu.SemaphoreType.DMA
    return pl.pallas_call(
        functools.partial(kernel, dims),
        out_shape=jax.ShapeDtypeStruct((toks, LANES), BF),
        in_specs=[vmem] * 5 + [hbm] * 3,
        out_specs=vmem,
        scratch_shapes=[
            pltpu.VMEM((2 * hid_pad, width), BF),
            pltpu.VMEM((hid_pad, width), BF),
            pltpu.VMEM((n_ep, toks), F32),
            pltpu.VMEM((toks, 8), F32),
            pltpu.VMEM((n_ep, cap, LANES), BF),
            pltpu.VMEM((n_tp, 8, LANES), F32),
            pltpu.VMEM((n_tp, n_ep * cap, LANES), BF),
            pltpu.VMEM((rows, width), BF),
            pltpu.VMEM((rows, hid_pad), BF),
            pltpu.VMEM((chunks, 2, nz, rows, LANES), BF),
            pltpu.VMEM((chunks, nz, rows, LANES), BF),
            pltpu.VMEM((chunks, 2, hops, rows, LANES), BF),
            pltpu.VMEM((chunks, 2, hops, rows, LANES), BF),
            pltpu.VMEM((n_ep * cap, LANES), BF),
            pltpu.VMEM((n_ep * cap, LANES), BF),
            pltpu.VMEM((2, toks, LANES), F32),
            pltpu.VMEM((n_tp, 1, toks), F32),
            pltpu.VMEM((1, toks), F32),
            dma((3,)),
            dma((n_tp,)), dma((n_tp,)),
            dma((n_ep,)), dma((n_ep,)),
            dma((chunks, 2, hops)), dma((chunks, 2, hops)),
            dma((chunks, nz)), dma((chunks, nz)),
            dma((chunks,)), dma((chunks,)),
            dma((chunks, 2, hops)), dma((chunks, 2, hops)),
            dma((n_ep,)), dma((n_ep,)),
            dma((n_tp,)), dma((n_tp,)),
        ],
        compiler_params=pltpu.CompilerParams(
            collective_id=0, has_side_effects=True, vmem_limit_bytes=66_000_000
        ),
        name="experts",
    )


def on_device(dims, tokens, pre_gain, ids, weights, gate_weight, up_weight, down_weight, post_gain):
    call = make(dims, tokens.shape[0], gate_weight.shape[2])
    return call(
        tokens, ids.T, weights.T, pre_gain[None], post_gain[None],
        gate_weight[0].T, up_weight[0].T, down_weight[0],
    )


def build(mesh, dims):
    placed = (
        P("ep", "tp"),
        P("tp"),
        P("ep", None),
        P("ep", None),
        P("ep", None, "tp"),
        P("ep", None, "tp"),
        P("ep", "tp", None),
        P("tp"),
    )
    return jax.shard_map(
        functools.partial(on_device, dims), mesh=mesh, in_specs=placed, out_specs=P("ep", "tp"), check_vma=False
    )


def solution(mesh):
    n_ep, n_tp = mesh.shape["ep"], mesh.shape["tp"]
    return build(mesh, (n_ep // NX, NX, n_tp // 2, 144, 2, 128 * n_tp))
```

time: 293 us -> 132 us (0.45)
  waiting for transfers between devices: 152 us -> 0 us
  Pallas kernels: 0 us -> 130 us
  local copies, waits for them, and re-layouts: 37.1 us -> 1.67 us
  matrix products: 28.4 us -> 0 us
  starting transfers between devices: 26.8 us -> 0 us
  blocking collectives: 18.3 us -> 0 us
  other arithmetic: 16.4 us -> 0 us
  between operations: 13.6 us -> 0.01 us
    pallas_call x0 -> x1, Pallas kernels: none -> 130 us  [on_device(): call(tokens, ids.T, weights.T, pre_gain[None], post_gain[None], gate_weig...]
    all_gather x1 -> x0, waiting for transfers between devices: 68.6 us -> none  [run_expert(): piece = lax.all_gather(routed, 'tp', axis=1, tiled=True)]
    unnamed x3 -> x0, waiting for transfers between devices: 66.5 us -> none
    dot_general x2 -> x0, matrix products: 28.4 us -> none  [the longest x1 17.7 us: run_expert(): jnp.dot(hidden, down_block, preferred_element_type=jnp.float32)]
    all_to_all x3 -> x0, starting transfers between devices: 26.6 us -> none  [the longest x2 19.8 us: copy_for_each(): lax.all_to_all(jnp.broadcast_to(value[None], (count, *value.shape)), axis...]
    unnamed x11 -> x1, local copies, waits for them, and re-layouts: 23.5 us -> 1.67 us
    all_to_all x1 -> x0, blocking collectives: 18.3 us -> none  [on_device(): lax.all_to_all(outgoing, 'ep', split_axis=0, concat_axis=0, tiled=True)]
    all_to_all x3 -> x0, waiting for transfers between devices: 16.8 us -> none  [the longest x1 9.08 us: on_device(): lax.all_to_all(results.reshape(groups, capacity, columns), 'ep', split_ax...]
  transfers between devices with their start and end apart: 5 -> 0, of which waited for: 4 -> 0; matrix products, arithmetic and copies ran while one was open for 6% -> 0% of each run, Pallas kernels for 0% -> 0%
where the time goes in v1:
time: 132 us
  Pallas kernels  130 us (98%)
  local copies, waits for them, and re-layouts  1.67 us (1%)
    pallas_call x1, Pallas kernels, on_device(): call(tokens, ids.T, weights.T, pre_gain[None], post_gain[None], gate_weig...  130 us

profile of v1, /device:TPU:1, one launch (start us, length us, event | category | flops | bytes accessed | tf_op | source)
XLA Modules:
  0.0 132.1 jit_solution(17258949360347498160)
XLA Ops:
  0.0 130.4 %experts.1 = bf16[1024,128]{1,0:T(8,128)(2,1)} custom-call(bf16[1024,128]{1,0:T(8,128)(2,1)} %tokens.1, s32[2,1024]{1,0:T(2,128)} %bitcast.14, f32[2,1024]{1,0:T(2,128)} %bitcast.15, bf16[1,128]{1,0:T(2,128)(2,1)} %bitcast.16, bf16[1,128]{1,0:T(2,128)(2,1)} %bitcast.17, bf16[448,2048]{1,0:T(8,128)(2,1)} %bitcast.11, bf16[448,2048]{1,0:T(8,128)(2,1)} %bitcast.12, ...), custom_call_target="tpu_custom_call" | custom-call | tf_op jit(solution)/shard_map/experts/pallas_call | solution.py:438
  130.4 1.7 %copy.10 = bf16[1024,128]{1,0:T(8,128)(2,1)} copy(bf16[1024,128]{1,0:T(8,128)(2,1)} %experts.1) | data formatting | bytes 524288

commit v2 on v1

v2 whole, which is shorter than its diff:
```python
import functools

import jax
import jax.numpy as jnp
from jax import lax
from jax.experimental import pallas as pl
from jax.experimental.pallas import tpu as pltpu
from jax.sharding import PartitionSpec as P

BF, F32 = jnp.bfloat16, jnp.float32
MESH = pl.DeviceIdType.MESH
NX = 4
EPS = 1e-06
LANES = 128
TURNS = 4
FOLD_AT = 1
NT = (((1,), (1,)), ((), ()))


def near_first(i, n):
    return i if n < 4 else i + lax.div(i, 2) - 2 * lax.div(i, 3)


def kernel(
    dims,
    tokens, ids, weights, pre_gain, post_gain, gate_hbm, up_hbm, down_hbm,
    out,
    gates, downs, ranks, cols, outgoing, gains, x_all, x_norm, hidden,
    part, peer_part, ring_out, ring_in, results, returned, sums, squares, square_own,
    tok_near, near_sums, near_out, near_in, row_scale,
    w_sem, gain_s, gain_r, disp_s, disp_r, ag_s, ag_r, d2d_s, d2d_r,
    pp_s, pp_r, rs_s, rs_r, ret_s, ret_r, sq_s, sq_r,
    tn_s, tn_r, near_s, near_r, nret_s, nret_r, nx_s, nx_r,
):
    ny, nx, nz, cap, per_chunk, width, plain_in, plain_out = dims
    n_ep, n_tp = ny * nx, nz * 2
    chunks = n_ep // per_chunk
    rows = cap * per_chunk
    near_out_chunks = chunks - plain_out
    half = -(-rows // 32) * 16
    hops = nz // 2
    toks = tokens.shape[0]
    hid = gate_hbm.shape[0]
    hid_pad = downs.shape[0]

    ep, tp = lax.axis_index("ep"), lax.axis_index("tp")
    y, x = lax.div(ep, nx), lax.rem(ep, nx)
    z, core = lax.div(tp, 2), lax.rem(tp, 2)
    peer = z * 2 + 1 - core
    right = lax.rem(z + 1, nz) * 2 + core
    left = lax.rem(z + nz - 1, nz) * 2 + core

    def remote(src, dst, ssem, rsem, ep_to, tp_to):
        return pltpu.make_async_remote_copy(
            src_ref=src, dst_ref=dst, send_sem=ssem, recv_sem=rsem,
            device_id=(ep_to, tp_to), device_id_type=MESH,
        )

    def arrived(ref, sem):
        pltpu.make_async_copy(ref, ref, sem).wait()

    barrier = pltpu.get_barrier_semaphore()

    def greet_ep(i, _):
        pl.semaphore_signal(barrier, inc=1, device_id=(lax.rem(ep + i, n_ep), tp), device_id_type=MESH)
        return 0

    def greet_tp(i, _):
        pl.semaphore_signal(barrier, inc=1, device_id=(ep, lax.rem(tp + i, n_tp)), device_id_type=MESH)
        return 0

    lax.fori_loop(1, n_ep, greet_ep, 0)
    lax.fori_loop(1, n_tp, greet_tp, 0)

    loads = (
        pltpu.make_async_copy(gate_hbm, gates.at[pl.ds(0, hid)], w_sem.at[0]),
        pltpu.make_async_copy(up_hbm, gates.at[pl.ds(hid_pad, hid)], w_sem.at[1]),
        pltpu.make_async_copy(down_hbm, downs.at[pl.ds(0, hid)], w_sem.at[2]),
    )
    for load in loads:
        load.start()
    if hid_pad > hid:
        gates[pl.ds(hid, hid_pad - hid), :] = jnp.zeros((hid_pad - hid, width), BF)
        gates[pl.ds(hid_pad + hid, hid_pad - hid), :] = jnp.zeros((hid_pad - hid, width), BF)
        downs[pl.ds(hid, hid_pad - hid), :] = jnp.zeros((hid_pad - hid, width), BF)
    gains[tp] = pre_gain[...].astype(F32)

    o_i = lax.broadcasted_iota(jnp.int32, (n_ep, toks), 0)
    a_i, b_i = o_i // nx, o_i % nx

    def near_vec(i, n):
        return i if n < 4 else jnp.where(i == 2, 3, jnp.where(i == 3, 2, i))

    e_of = ((y + near_vec(a_i, ny)) % ny) * nx + (x + near_vec(b_i, nx)) % nx
    first = (ids[0:1, :] == e_of).astype(F32)
    second = (ids[1:2, :] == e_of).astype(F32)
    named = first + second
    named_bf = named.astype(BF)
    step = min(256, toks)
    for at in range(0, toks, step):
        before = lax.broadcasted_iota(jnp.int32, (toks, step), 0)
        after = lax.broadcasted_iota(jnp.int32, (toks, step), 1) + at
        upper = jnp.where(before < after, 1.0, 0.0).astype(BF)
        ranks[:, pl.ds(at, step)] = jnp.dot(named_bf, upper, preferred_element_type=F32)
    rank = ranks[...]
    slot = o_i.astype(F32) * float(cap) + rank
    slot0 = jnp.sum(first * slot, axis=0, keepdims=True)
    slot1 = jnp.sum(second * slot, axis=0, keepdims=True)
    ranks[...] = jnp.where(named > 0.0, rank, -1.0)
    r8 = lax.broadcasted_iota(jnp.int32, (8, toks), 0)
    table = jnp.where(r8 == 0, slot0, jnp.where(r8 == 1, slot1, jnp.where(r8 == 2, weights[0:1, :], weights[1:2, :])))
    cols[...] = table.T

    def block_peer(o, sign):
        dy = near_first(lax.div(o, nx), ny)
        dx = near_first(lax.rem(o, nx), nx)
        return lax.rem(y + ny + sign * dy, ny) * nx + lax.rem(x + nx + sign * dx, nx)

    def block_rows(o):
        return pl.ds(pl.multiple_of(o * cap, 16), cap)

    def dispatch_copy(o):
        return remote(
            outgoing.at[0, o], x_all.at[tp, block_rows(o)], disp_s, disp_r.at[o], block_peer(o, 1), tp
        )

    s_i = lax.broadcasted_iota(jnp.int32, (cap, toks), 0).astype(F32)

    def dispatch(o, _):
        pick = jnp.where(s_i == ranks[pl.ds(o, 1), :], 1.0, 0.0).astype(BF)
        picked = jnp.dot(pick, tokens[...], preferred_element_type=F32).astype(BF)

        @pl.when(o == 0)
        def _():
            x_all[tp, pl.ds(0, cap)] = picked

        @pl.when(o > 0)
        def _():
            outgoing[0, o] = picked

        return 0

    lax.fori_loop(0, n_ep, dispatch, 0)

    pl.semaphore_wait(barrier, n_ep - 1 + n_tp - 1)

    def send_gain(i, _):
        remote(gains.at[tp], gains.at[tp], gain_s, gain_r, ep, lax.rem(tp + i, n_tp)).start()
        return 0

    def token_copy(way):
        return remote(
            tokens, tok_near.at[way], tn_s.at[way], tn_r.at[way], ep, right if way == 0 else left
        )

    def send_block(o, _):
        dispatch_copy(o).start()
        return 0

    if plain_in < chunks:
        for way in (0, 1):
            token_copy(way).start()
    lax.fori_loop(1, n_ep, send_block, 0)
    lax.fori_loop(1, n_tp, send_gain, 0)

    def chunk_rows(c, at=0, count=None):
        return pl.ds(pl.multiple_of(c * rows + at, 16), rows if count is None else count)

    def slice_at(h):
        return lax.rem(z + 2 * nz - h, nz) * 2 + core

    def ag_copy(c, h, way):
        j = slice_at(h - 1 if way == 0 else 1 - h)
        at, count = (0, rows) if h < hops else ((0, half) if way == 0 else (half, rows - half))
        ref = x_all.at[j, chunk_rows(c, at, count)]
        return remote(ref, ref, ag_s.at[c], ag_r.at[lax.rem(c, TURNS), way, h - 1], ep, right if way == 0 else left)

    def ag_arrived(c, h, way):
        j = slice_at(h if way == 0 else -h)
        at, count = (0, rows) if h < hops else ((0, half) if way == 0 else (half, rows - half))
        ref = x_all.at[j, chunk_rows(c, at, count)]
        remote(ref, ref, ag_s.at[c], ag_r.at[lax.rem(c, TURNS), way, h - 1], ep, right).wait_recv()

    def d2d_copy(c, q):
        ref = x_all.at[slice_at(q), chunk_rows(c)]
        return remote(ref, ref, d2d_s, d2d_r.at[c], ep, peer)

    def near_copy(o, way):
        j = slice_at(1 if way == 0 else -1)
        return remote(
            outgoing.at[1 + way, o], x_all.at[j, block_rows(o)],
            near_s, near_r.at[lax.div(o, per_chunk)], block_peer(o, 1), tp,
        )

    def near_dispatch(c):
        @pl.when(c == plain_in)
        def _():
            for way in (0, 1):
                token_copy(way).wait_recv()

        for b in range(per_chunk):
            o = c * per_chunk + b
            pick = jnp.where(s_i == ranks[pl.ds(o, 1), :], 1.0, 0.0).astype(BF)
            both = jnp.concatenate([tok_near[0], tok_near[1]], axis=1)
            picked = jnp.dot(pick, both, preferred_element_type=F32).astype(BF)
            for way in (0, 1):
                outgoing[1 + way, o] = picked[:, way * LANES:(way + 1) * LANES]
                near_copy(o, way).start()

    def gather_first(c):
        for b in range(per_chunk):
            o = c * per_chunk + b

            @pl.when(o > 0)
            def _():
                dispatch_copy(o).wait_recv()

        @pl.when(c < plain_in)
        def _():
            ag_copy(c, 1, 0).start()
            ag_copy(c, 1, 1).start()

        d2d_copy(c, 0).start()

    def gather_hop(c, h):
        if h == 1:
            @pl.when(c >= plain_in)
            def _():
                arrived(x_all.at[pl.ds(0, 2), chunk_rows(c)], near_r.at[c])

        for way in (0, 1):
            if h > 1:
                ag_arrived(c, h, way)
            else:
                @pl.when(c < plain_in)
                def _():
                    ag_arrived(c, h, way)

            if h < hops:
                ag_copy(c, h + 1, way).start()
                d2d_copy(c, h if way == 0 else -h).start()
        if h == hops:
            d2d_copy(c, h).start()

    def fold_gain():
        for load in loads:
            load.wait()
        arrived(gains.at[pl.ds(1, n_tp - 1)], gain_r)
        gain = jnp.concatenate([gains[j] for j in range(n_tp)], axis=1)
        block = 64

        def fold(i, _):
            at = pl.ds(pl.multiple_of(i * block, block), block)
            gates[at, :] = (gates[at, :].astype(F32) * gain).astype(BF)
            return 0

        lax.fori_loop(0, 2 * hid_pad // block, fold, 0)

    def feed_forward(c):
        arrived(x_all.at[pl.ds(0, nz), chunk_rows(c)], d2d_r.at[c])

        def squares_of(i, _):
            at = pl.ds(pl.multiple_of(c * rows + i * 16, 16), 16)
            to = pl.ds(pl.multiple_of(i * 16, 16), 16)
            total = jnp.zeros((16, LANES), F32)
            for j in range(n_tp):
                raw = x_all[j, at]
                x_norm[to, j * LANES:(j + 1) * LANES] = raw
                v = raw.astype(F32)
                total = total + v * v
            mean = jnp.sum(total, axis=1, keepdims=True) / width
            row_scale[to, :] = jnp.broadcast_to(lax.rsqrt(mean + EPS), (16, LANES))
            return 0

        lax.fori_loop(0, rows // 16, squares_of, 0, unroll=3 if rows % 48 == 0 else 1)
        tile = min(256, hid_pad)
        for at in range(0, hid_pad, tile):
            g = lax.dot_general(x_norm[...], gates[at:at + tile, :], NT, preferred_element_type=F32)
            u = lax.dot_general(x_norm[...], gates[hid_pad + at:hid_pad + at + tile, :], NT, preferred_element_type=F32)
            scale = jnp.concatenate([row_scale[...]] * (tile // LANES), axis=1)
            g, u = g * scale, u * scale
            hidden[:, at:at + tile] = (g / (1.0 + jnp.exp(-g)) * u).astype(BF)

        for m in range(nz):
            p = jnp.dot(hidden[...], downs[:, m * 256:(m + 1) * 256], preferred_element_type=F32).astype(BF)
            part[c, 0, m] = p[:, :LANES]
            part[c, 1, m] = p[:, LANES:]
        peer_copy(c).start()

    def peer_copy(c):
        return remote(part.at[c, 1 - core], peer_part.at[c], pp_s, pp_r.at[lax.rem(c, TURNS)], ep, peer)

    def chip_sum(c, zd, at=0, count=None):
        sl = pl.ds(at, rows if count is None else count)
        return part[c, core, zd, sl, :].astype(F32) + peer_part[c, zd, sl, :].astype(F32)

    def rs_copy(c, s, way):
        at, count = (0, rows) if s > 1 else ((0, half) if way == 0 else (half, rows - half))
        sl = pl.ds(at, count)
        return remote(
            ring_out.at[c, way, s - 1, sl], ring_in.at[c, way, s - 1, sl],
            rs_s.at[c], rs_r.at[lax.rem(c, TURNS), way, s - 1], ep, right if way == 0 else left,
        )

    def scatter_stage(c, s):
        if s == 1:
            peer_copy(c).wait_recv()
        for way in (0, 1):
            far = hops + 1 - s
            zd = lax.rem(z + far, nz) if way == 0 else lax.rem(z + nz - far, nz)
            if s == 1:
                at = 0 if way == 0 else half
                count = half if way == 0 else rows - half
                ring_out[c, way, 0, at:at + count, :] = chip_sum(c, zd, at, count).astype(BF)
            else:
                rs_copy(c, s - 1, way).wait_recv()
                for at, count in ((0, half), (half, rows - half)):
                    v = chip_sum(c, zd, at, count)
                    if s > 2 or (at == 0) == (way == 0):
                        v = v + ring_in[c, way, s - 2, at:at + count, :].astype(F32)
                    ring_out[c, way, s - 1, at:at + count, :] = v.astype(BF)
            rs_copy(c, s, way).start()

    def return_copy(o):
        return remote(
            results.at[0, block_rows(o)], returned.at[0, block_rows(o)], ret_s, ret_r.at[o], block_peer(o, -1), tp
        )

    def near_return_copy(o, way):
        return remote(
            results.at[1 + way, block_rows(o)], returned.at[1 + way, block_rows(o)],
            nret_s, nret_r.at[lax.div(o, per_chunk)], block_peer(o, -1), tp,
        )

    def last_hop(c):
        @pl.when(c >= near_out_chunks)
        def _():
            scatter_stage(c, hops)

        @pl.when(c < near_out_chunks)
        def _():
            for way in (0, 1):
                rs_copy(c, hops - 1, way).wait_recv()
            for b in range(per_chunk):
                o = c * per_chunk + b
                at = b * cap
                own = chip_sum(c, z, at, cap).astype(BF)
                near = []
                for way in (0, 1):
                    zd = lax.rem(z + 1, nz) if way == 0 else lax.rem(z + nz - 1, nz)
                    v = chip_sum(c, zd, at, cap) + ring_in[c, way, hops - 2, at:at + cap, :].astype(F32)
                    near.append(v.astype(BF))

                @pl.when(o == 0)
                def _():
                    returned[0, pl.ds(0, cap), :] = own
                    for way in (0, 1):
                        returned[1 + way, pl.ds(0, cap), :] = near[way]

                @pl.when(o > 0)
                def _():
                    results[0, block_rows(o), :] = own
                    return_copy(o).start()
                    for way in (0, 1):
                        results[1 + way, block_rows(o), :] = near[way]
                        near_return_copy(o, way).start()

    def finish(c):
        @pl.when(c < near_out_chunks)
        def _():
            combine(c, True)

        @pl.when(c >= near_out_chunks)
        def _():
            for way in (0, 1):
                rs_copy(c, hops, way).wait_recv()
            for b in range(per_chunk):
                o = c * per_chunk + b
                at = b * cap
                v = chip_sum(c, z, at, cap)
                for way in (0, 1):
                    v = v + ring_in[c, way, hops - 1, at:at + cap, :].astype(F32)
                v = v.astype(BF)

                @pl.when(o == 0)
                def _():
                    returned[0, pl.ds(0, cap), :] = v

                @pl.when(o > 0)
                def _():
                    results[0, block_rows(o), :] = v
                    return_copy(o).start()

    def near_sum_copy(way):
        return remote(
            near_out.at[way], near_in.at[way], nx_s.at[way], nx_r.at[way], ep, right if way == 0 else left
        )

    def combine(c, near):
        for b in range(per_chunk):
            o = c * per_chunk + b

            @pl.when(o > 0)
            def _():
                return_copy(o).wait_recv()

        lane = lax.broadcasted_iota(jnp.int32, (toks, rows), 1).astype(F32) + (c * rows).astype(F32)
        values = returned[0, chunk_rows(c), :]
        if near:
            @pl.when(c > 0)
            def _():
                arrived(x_all.at[pl.ds(0, 2), chunk_rows(c)], nret_r.at[c])

            @pl.when(c == 0)
            def _():
                if per_chunk > 1:
                    arrived(x_all.at[pl.ds(0, 2), pl.ds(0, rows - cap)], nret_r.at[c])

            values = jnp.concatenate([values, returned[1, chunk_rows(c), :], returned[2, chunk_rows(c), :]], axis=1)
        for k in (0, 1):
            pick = jnp.where(lane == cols[:, k:k + 1], 1.0, 0.0).astype(BF)
            got = jnp.dot(pick, values, preferred_element_type=F32)

            @pl.when(c == 0)
            def _():
                sums[k] = got[:, :LANES]
                if near:
                    near_sums[k] = got[:, LANES:]

            @pl.when(c > 0)
            def _():
                sums[k] = sums[k] + got[:, :LANES]
                if near:
                    near_sums[k] = near_sums[k] + got[:, LANES:]

        if near:
            @pl.when(c == near_out_chunks - 1)
            def _():
                total = cols[:, 2:3] * near_sums[0] + cols[:, 3:4] * near_sums[1]
                for way in (0, 1):
                    near_out[way] = total[:, way * LANES:(way + 1) * LANES].astype(BF)
                    near_sum_copy(way).start()

    def last_combine(c):
        @pl.when(c >= near_out_chunks)
        def _():
            combine(c, False)

    stages = [(gather_first, 0)]
    if plain_in < chunks:
        stages += [(near_dispatch, -1)]
    stages += [(functools.partial(gather_hop, h=h), h) for h in range(1, hops + 1)]
    stages += [(feed_forward, hops + 1)]
    stages += [(functools.partial(scatter_stage, s=s), hops + 1 + s) for s in range(1, hops)]
    stages += [(last_hop, 2 * hops + 1), (finish, 2 * hops + 2), (last_combine, 2 * hops + 3)]

    def slot_step(t, _):
        @pl.when(t == FOLD_AT)
        def _():
            fold_gain()

        for stage, first_slot in stages:
            c = t - first_slot
            low = plain_in if stage is near_dispatch else 0

            @pl.when((c >= low) & (c < chunks))
            def _():
                stage(c)

        return 0

    lax.fori_loop(0, chunks + 2 * hops + 3, slot_step, 0)

    both = cols[:, 2:3] * sums[0] + cols[:, 3:4] * sums[1]
    if near_out_chunks:
        for way in (0, 1):
            near_sum_copy(way).wait_recv()
            both = both + near_in[way].astype(F32)
    sums[0] = both
    square_own[...] = jnp.sum((both * both).T, axis=0, keepdims=True)

    def square_copy(i):
        return remote(square_own, squares.at[i], sq_s, sq_r, ep, lax.rem(tp + i, n_tp))

    def send_square(i, _):
        square_copy(i).start()
        return 0

    lax.fori_loop(1, n_tp, send_square, 0)

    arrived(gains.at[pl.ds(1, n_tp - 1)], gain_s)
    arrived(outgoing.at[0, pl.ds(1, n_ep - 1)], disp_s)
    arrived(results.at[0, pl.ds(cap, (n_ep - 1) * cap)], ret_s)
    arrived(x_all.at[pl.ds(0, nz)], d2d_s)
    arrived(x_all.at[pl.ds(0, nz)], pp_s)
    for c in range(chunks):
        arrived(part.at[c, 0, pl.ds(0, nz - 1 if c < plain_in else nz - 3)], ag_s.at[c])
        arrived(part.at[c, 0, pl.ds(0, nz - 3 if c < near_out_chunks else nz - 1)], rs_s.at[c])
    first_near = plain_in * per_chunk
    if first_near < n_ep:
        arrived(outgoing.at[pl.ds(1, 2), pl.ds(first_near, n_ep - first_near)], near_s)
    last_near = near_out_chunks * per_chunk
    if last_near > 1:
        arrived(results.at[pl.ds(1, 2), pl.ds(cap, (last_near - 1) * cap)], nret_s)
    for way in (0, 1):
        if plain_in < chunks:
            token_copy(way).wait_send()
        if near_out_chunks:
            near_sum_copy(way).wait_send()

    total = square_own[...]
    arrived(squares.at[pl.ds(1, n_tp - 1)], sq_r)
    for i in range(1, n_tp):
        total = total + squares[i]
    scale = lax.rsqrt(total / width + EPS)
    scale = jnp.broadcast_to(scale, (8, toks)).T
    out[...] = (sums[0] * scale[:, 0:1] * post_gain[...].astype(F32)).astype(BF)

    arrived(squares.at[pl.ds(1, n_tp - 1)], sq_s)


def make(dims, toks, hid):
    ny, nx, nz, cap, per_chunk, width, _, _ = dims
    n_ep, n_tp = ny * nx, nz * 2
    chunks, rows, hops = n_ep // per_chunk, cap * per_chunk, nz // 2
    hid_pad = -(-hid // 256) * 256 if hid > 128 else 128
    vmem = pl.BlockSpec(memory_space=pltpu.VMEM)
    hbm = pl.BlockSpec(memory_space=pl.ANY)
    dma = pltpu.SemaphoreType.DMA
    return pl.pallas_call(
        functools.partial(kernel, dims),
        out_shape=jax.ShapeDtypeStruct((toks, LANES), BF),
        in_specs=[vmem] * 5 + [hbm] * 3,
        out_specs=vmem,
        scratch_shapes=[
            pltpu.VMEM((2 * hid_pad, width), BF),
            pltpu.VMEM((hid_pad, width), BF),
            pltpu.VMEM((n_ep, toks), F32),
            pltpu.VMEM((toks, 8), F32),
            pltpu.VMEM((3, n_ep, cap, LANES), BF),
            pltpu.VMEM((n_tp, 1, LANES), F32),
            pltpu.VMEM((n_tp, n_ep * cap, LANES), BF),
            pltpu.VMEM((rows, width), BF),
            pltpu.VMEM((rows, hid_pad), BF),
            pltpu.VMEM((chunks, 2, nz, rows, LANES), BF),
            pltpu.VMEM((chunks, nz, rows, LANES), BF),
            pltpu.VMEM((chunks, 2, hops, rows, LANES), BF),
            pltpu.VMEM((chunks, 2, hops, rows, LANES), BF),
            pltpu.VMEM((3, n_ep * cap, LANES), BF),
            pltpu.VMEM((3, n_ep * cap, LANES), BF),
            pltpu.VMEM((2, toks, LANES), F32),
            pltpu.VMEM((n_tp, 1, toks), F32),
            pltpu.VMEM((1, toks), F32),
            pltpu.VMEM((2, toks, LANES), BF),
            pltpu.VMEM((2, toks, 2 * LANES), F32),
            pltpu.VMEM((2, toks, LANES), BF),
            pltpu.VMEM((2, toks, LANES), BF),
            pltpu.VMEM((rows, LANES), F32),
            dma((3,)),
            dma, dma,
            dma, dma((n_ep,)),
            dma((chunks,)), dma((TURNS, 2, hops)), dma, dma((chunks,)),
            dma, dma((TURNS,)),
            dma((chunks,)), dma((TURNS, 2, hops)),
            dma, dma((n_ep,)),
            dma, dma,
            dma((2,)), dma((2,)),
            dma, dma((chunks,)),
            dma, dma((chunks,)),
            dma((2,)), dma((2,)),
        ],
        compiler_params=pltpu.CompilerParams(
            collective_id=0, has_side_effects=True, vmem_limit_bytes=66_000_000
        ),
        name="experts",
    )


def on_device(dims, tokens, pre_gain, ids, weights, gate_weight, up_weight, down_weight, post_gain):
    call = make(dims, tokens.shape[0], gate_weight.shape[2])
    return call(
        tokens, ids.T, weights.T, pre_gain[None], post_gain[None],
        gate_weight[0].T, up_weight[0].T, down_weight[0],
    )


def build(mesh, dims):
    placed = (
        P("ep", "tp"),
        P("tp"),
        P("ep", None),
        P("ep", None),
        P("ep", None, "tp"),
        P("ep", None, "tp"),
        P("ep", "tp", None),
        P("tp"),
    )
    return jax.shard_map(
        functools.partial(on_device, dims), mesh=mesh, in_specs=placed, out_specs=P("ep", "tp"), check_vma=False
    )


def solution(mesh):
    n_ep, n_tp = mesh.shape["ep"], mesh.shape["tp"]
    return build(mesh, (n_ep // NX, NX, n_tp // 2, 144, 2, 128 * n_tp, 8, 8))
```

time: 132 us -> 127 us (0.962)
  Pallas kernels: 130 us -> 126 us
    pallas_call x1, Pallas kernels: 130 us -> 126 us  [on_device(): call(tokens, ids.T, weights.T, pre_gain[None], post_gain[None], gate_weig...]
where the time goes in v2:
time: 127 us
  Pallas kernels  126 us (99%)
  local copies, waits for them, and re-layouts  1.67 us (1%)
    pallas_call x1, Pallas kernels, on_device(): call(tokens, ids.T, weights.T, pre_gain[None], post_gain[None], gate_weig...  126 us

profile of v2, /device:TPU:1, one launch (start us, length us, event | category | flops | bytes accessed | tf_op | source)
XLA Modules:
  0.0 127.3 jit_solution(8981283212960350700)
XLA Ops:
  0.0 125.7 %experts.1 = bf16[1024,128]{1,0:T(8,128)(2,1)} custom-call(bf16[1024,128]{1,0:T(8,128)(2,1)} %tokens.1, s32[2,1024]{1,0:T(2,128)} %bitcast.14, f32[2,1024]{1,0:T(2,128)} %bitcast.15, bf16[1,128]{1,0:T(2,128)(2,1)} %bitcast.16, bf16[1,128]{1,0:T(2,128)(2,1)} %bitcast.17, bf16[448,2048]{1,0:T(8,128)(2,1)} %bitcast.11, bf16[448,2048]{1,0:T(8,128)(2,1)} %bitcast.12, ...), custom_call_target="tpu_custom_call" | custom-call | tf_op jit(solution)/shard_map/experts/pallas_call | solution.py:581
  125.7 1.7 %copy.10 = bf16[1024,128]{1,0:T(8,128)(2,1)} copy(bf16[1024,128]{1,0:T(8,128)(2,1)} %experts.1) | data formatting | bytes 524288

commit v3 on v2

--- a/solution.py
+++ b/solution.py
@@ -169,17 +169,21 @@
     def slice_at(h):
         return lax.rem(z + 2 * nz - h, nz) * 2 + core
 
-    def ag_copy(c, h, way):
-        j = slice_at(h - 1 if way == 0 else 1 - h)
-        at, count = (0, rows) if h < hops else ((0, half) if way == 0 else (half, rows - half))
-        ref = x_all.at[j, chunk_rows(c, at, count)]
-        return remote(ref, ref, ag_s.at[c], ag_r.at[lax.rem(c, TURNS), way, h - 1], ep, right if way == 0 else left)
-
-    def ag_arrived(c, h, way):
-        j = slice_at(h if way == 0 else -h)
-        at, count = (0, rows) if h < hops else ((0, half) if way == 0 else (half, rows - half))
-        ref = x_all.at[j, chunk_rows(c, at, count)]
-        remote(ref, ref, ag_s.at[c], ag_r.at[lax.rem(c, TURNS), way, h - 1], ep, right).wait_recv()
+    def sub_rows(sub):
+        return (0, half) if sub == 0 else (half, rows - half)
+
+    def subs_of(h, way):
+        return (0, 1) if h < hops else (way,)
+
+    def ag_copy(c, h, way, sub):
+        ref = x_all.at[slice_at(h - 1 if way == 0 else 1 - h), chunk_rows(c, *sub_rows(sub))]
+        return remote(
+            ref, ref, ag_s.at[c], ag_r.at[lax.rem(c, TURNS), way, h - 1, sub], ep, right if way == 0 else left
+        )
+
+    def ag_arrived(c, h, way, sub):
+        ref = x_all.at[slice_at(h if way == 0 else -h), chunk_rows(c, *sub_rows(sub))]
+        remote(ref, ref, ag_s.at[c], ag_r.at[lax.rem(c, TURNS), way, h - 1, sub], ep, right).wait_recv()
 
     def d2d_copy(c, q):
         ref = x_all.at[slice_at(q), chunk_rows(c)]
@@ -215,10 +219,15 @@
             def _():
                 dispatch_copy(o).wait_recv()
 
-        @pl.when(c < plain_in)
-        def _():
-            ag_copy(c, 1, 0).start()
-            ag_copy(c, 1, 1).start()
+            if (b + 1) * cap in (half, rows):
+                sub = 0 if (b + 1) * cap == half else 1
+
+                @pl.when(c < plain_in)
+                def _():
+                    for way in (0, 1):
+                        for piece in ((0, 1) if per_chunk == 1 else (sub,)):
+                            ag_copy(c, 1, way, piece).start()
+
 
         d2d_copy(c, 0).start()
 
@@ -228,17 +237,22 @@
             def _():
                 arrived(x_all.at[pl.ds(0, 2), chunk_rows(c)], near_r.at[c])
 
-        for way in (0, 1):
-            if h > 1:
-                ag_arrived(c, h, way)
-            else:
-                @pl.when(c < plain_in)
-                def _():
-                    ag_arrived(c, h, way)
-
-            if h < hops:
-                ag_copy(c, h + 1, way).start()
-                d2d_copy(c, h if way == 0 else -h).start()
+        for sub in (0, 1):
+            for way in (0, 1):
+                if sub not in subs_of(h, way):
+                    continue
+                if h > 1:
+                    ag_arrived(c, h, way, sub)
+                else:
+                    @pl.when(c < plain_in)
+                    def _():
+                        ag_arrived(c, h, way, sub)
+
+                if h < hops and sub in subs_of(h + 1, way):
+                    ag_copy(c, h + 1, way, sub).start()
+                if h < hops and sub == 1:
+                    d2d_copy(c, h if way == 0 else -h).start()
+
         if h == hops:
             d2d_copy(c, h).start()
 
@@ -273,14 +287,16 @@
             return 0
 
         lax.fori_loop(0, rows // 16, squares_of, 0, unroll=3 if rows % 48 == 0 else 1)
-        tile = min(256, hid_pad)
-        for at in range(0, hid_pad, tile):
-            g = lax.dot_general(x_norm[...], gates[at:at + tile, :], NT, preferred_element_type=F32)
-            u = lax.dot_general(x_norm[...], gates[hid_pad + at:hid_pad + at + tile, :], NT, preferred_element_type=F32)
-            scale = jnp.concatenate([row_scale[...]] * (tile // LANES), axis=1)
-            g, u = g * scale, u * scale
-            hidden[:, at:at + tile] = (g / (1.0 + jnp.exp(-g)) * u).astype(BF)
-
+    tile = min(256, hid_pad)
+
+    def project(c, at):
+        g = lax.dot_general(x_norm[...], gates[at:at + tile, :], NT, preferred_element_type=F32)
+        u = lax.dot_general(x_norm[...], gates[hid_pad + at:hid_pad + at + tile, :], NT, preferred_element_type=F32)
+        scale = jnp.concatenate([row_scale[...]] * (tile // LANES), axis=1)
+        g, u = g * scale, u * scale
+        hidden[:, at:at + tile] = (g / (1.0 + jnp.exp(-g)) * u).astype(BF)
+
+    def project_down(c):
         for m in range(nz):
             p = jnp.dot(hidden[...], downs[:, m * 256:(m + 1) * 256], preferred_element_type=F32).astype(BF)
             part[c, 0, m] = p[:, :LANES]
@@ -294,32 +310,38 @@
         sl = pl.ds(at, rows if count is None else count)
         return part[c, core, zd, sl, :].astype(F32) + peer_part[c, zd, sl, :].astype(F32)
 
-    def rs_copy(c, s, way):
-        at, count = (0, rows) if s > 1 else ((0, half) if way == 0 else (half, rows - half))
-        sl = pl.ds(at, count)
+    def rs_subs(s, way):
+        return (0, 1) if s > 1 else (way,)
+
+    def rs_copy(c, s, way, sub):
+        sl = pl.ds(*sub_rows(sub))
         return remote(
             ring_out.at[c, way, s - 1, sl], ring_in.at[c, way, s - 1, sl],
-            rs_s.at[c], rs_r.at[lax.rem(c, TURNS), way, s - 1], ep, right if way == 0 else left,
+            rs_s.at[c], rs_r.at[lax.rem(c, TURNS), way, s - 1, sub], ep, right if way == 0 else left,
         )
 
     def scatter_stage(c, s):
         if s == 1:
             peer_copy(c).wait_recv()
-        for way in (0, 1):
-            far = hops + 1 - s
-            zd = lax.rem(z + far, nz) if way == 0 else lax.rem(z + nz - far, nz)
-            if s == 1:
-                at = 0 if way == 0 else half
-                count = half if way == 0 else rows - half
-                ring_out[c, way, 0, at:at + count, :] = chip_sum(c, zd, at, count).astype(BF)
-            else:
-                rs_copy(c, s - 1, way).wait_recv()
-                for at, count in ((0, half), (half, rows - half)):
-                    v = chip_sum(c, zd, at, count)
-                    if s > 2 or (at == 0) == (way == 0):
-                        v = v + ring_in[c, way, s - 2, at:at + count, :].astype(F32)
-                    ring_out[c, way, s - 1, at:at + count, :] = v.astype(BF)
-            rs_copy(c, s, way).start()
+        far = hops + 1 - s
+        for sub in (0, 1):
+            at, count = sub_rows(sub)
+            for way in (0, 1):
+                if sub not in rs_subs(s, way):
+                    continue
+                zd = lax.rem(z + far, nz) if way == 0 else lax.rem(z + nz - far, nz)
+                v = chip_sum(c, zd, at, count)
+                if s > 1 and sub in rs_subs(s - 1, way):
+                    rs_copy(c, s - 1, way, sub).wait_recv()
+                    v = v + ring_in[c, way, s - 2, at:at + count, :].astype(F32)
+                ring_out[c, way, s - 1, at:at + count, :] = v.astype(BF)
+                rs_copy(c, s, way, sub).start()
+
+    def stage_arrived(c, s):
+        for sub in (0, 1):
+            for way in (0, 1):
+                if sub in rs_subs(s, way):
+                    rs_copy(c, s, way, sub).wait_recv()
 
     def return_copy(o):
         return remote(
@@ -339,8 +361,7 @@
 
         @pl.when(c < near_out_chunks)
         def _():
-            for way in (0, 1):
-                rs_copy(c, hops - 1, way).wait_recv()
+            stage_arrived(c, hops - 1)
             for b in range(per_chunk):
                 o = c * per_chunk + b
                 at = b * cap
@@ -372,8 +393,7 @@
 
         @pl.when(c >= near_out_chunks)
         def _():
-            for way in (0, 1):
-                rs_copy(c, hops, way).wait_recv()
+            stage_arrived(c, hops)
             for b in range(per_chunk):
                 o = c * per_chunk + b
                 at = b * cap
@@ -449,8 +469,12 @@
     stages = [(gather_first, 0)]
     if plain_in < chunks:
         stages += [(near_dispatch, -1)]
-    stages += [(functools.partial(gather_hop, h=h), h) for h in range(1, hops + 1)]
-    stages += [(feed_forward, hops + 1)]
+    hop = [(functools.partial(gather_hop, h=h), h) for h in range(1, hops + 1)]
+    forward = [feed_forward] + [functools.partial(project, at=at) for at in range(0, hid_pad, tile)] + [project_down]
+    forward = [(part_of, hops + 1) for part_of in forward]
+    while hop or forward:
+        stages += hop[:1] + forward[:1]
+        hop, forward = hop[1:], forward[1:]
     stages += [(functools.partial(scatter_stage, s=s), hops + 1 + s) for s in range(1, hops)]
     stages += [(last_hop, 2 * hops + 1), (finish, 2 * hops + 2), (last_combine, 2 * hops + 3)]
 
@@ -559,9 +583,9 @@
             dma((3,)),
             dma, dma,
             dma, dma((n_ep,)),
-            dma((chunks,)), dma((TURNS, 2, hops)), dma, dma((chunks,)),
+            dma((chunks,)), dma((TURNS, 2, hops, 2)), dma, dma((chunks,)),
             dma, dma((TURNS,)),
-            dma((chunks,)), dma((TURNS, 2, hops)),
+            dma((chunks,)), dma((TURNS, 2, hops, 2)),
             dma, dma((n_ep,)),
             dma, dma,
             dma((2,)), dma((2,)),
@@ -602,4 +626,4 @@
 
 def solution(mesh):
     n_ep, n_tp = mesh.shape["ep"], mesh.shape["tp"]
-    return build(mesh, (n_ep // NX, NX, n_tp // 2, 144, 2, 128 * n_tp, 8, 8))
+    return build(mesh, (n_ep // NX, NX, n_tp // 2, 144, 2, 128 * n_tp, 2, 8))

time: 127 us -> 126 us (level)
  no operation moved by 1% of the time
where the time goes in v3:
time: 126 us
  Pallas kernels  125 us (99%)
  local copies, waits for them, and re-layouts  1.67 us (1%)
    pallas_call x1, Pallas kernels, on_device(): call(tokens, ids.T, weights.T, pre_gain[None], post_gain[None], gate_weig...  125 us

profile of v3, /device:TPU:1, one launch (start us, length us, event | category | flops | bytes accessed | tf_op | source)
XLA Modules:
  0.0 126.2 jit_solution(13759122413727266119)
XLA Ops:
  0.0 124.5 %experts.1 = bf16[1024,128]{1,0:T(8,128)(2,1)} custom-call(bf16[1024,128]{1,0:T(8,128)(2,1)} %tokens.1, s32[2,1024]{1,0:T(2,128)} %bitcast.14, f32[2,1024]{1,0:T(2,128)} %bitcast.15, bf16[1,128]{1,0:T(2,128)(2,1)} %bitcast.16, bf16[1,128]{1,0:T(2,128)(2,1)} %bitcast.17, bf16[448,2048]{1,0:T(8,128)(2,1)} %bitcast.11, bf16[448,2048]{1,0:T(8,128)(2,1)} %bitcast.12, ...), custom_call_target="tpu_custom_call" | custom-call | tf_op jit(solution)/shard_map/experts/pallas_call | solution.py:605
  124.5 1.7 %copy.10 = bf16[1024,128]{1,0:T(8,128)(2,1)} copy(bf16[1024,128]{1,0:T(8,128)(2,1)} %experts.1) | data formatting | bytes 524288

commit v4 on v3

--- a/solution.py
+++ b/solution.py
@@ -467,14 +467,14 @@
             combine(c, False)
 
     stages = [(gather_first, 0)]
-    if plain_in < chunks:
-        stages += [(near_dispatch, -1)]
     hop = [(functools.partial(gather_hop, h=h), h) for h in range(1, hops + 1)]
     forward = [feed_forward] + [functools.partial(project, at=at) for at in range(0, hid_pad, tile)] + [project_down]
     forward = [(part_of, hops + 1) for part_of in forward]
     while hop or forward:
         stages += hop[:1] + forward[:1]
         hop, forward = hop[1:], forward[1:]
+    if plain_in < chunks:
+        stages += [(near_dispatch, -1)]
     stages += [(functools.partial(scatter_stage, s=s), hops + 1 + s) for s in range(1, hops)]
     stages += [(last_hop, 2 * hops + 1), (finish, 2 * hops + 2), (last_combine, 2 * hops + 3)]
 

time: 126 us -> 126 us (level)
  no operation moved by 1% of the time
where the time goes in v4:
time: 126 us
  Pallas kernels  125 us (99%)
  local copies, waits for them, and re-layouts  1.67 us (1%)
    pallas_call x1, Pallas kernels, on_device(): call(tokens, ids.T, weights.T, pre_gain[None], post_gain[None], gate_weig...  125 us

profile of v4, /device:TPU:1, one launch (start us, length us, event | category | flops | bytes accessed | tf_op | source)
XLA Modules:
  0.0 126.3 jit_solution(9702497325245778331)
XLA Ops:
  0.0 124.6 %experts.1 = bf16[1024,128]{1,0:T(8,128)(2,1)} custom-call(bf16[1024,128]{1,0:T(8,128)(2,1)} %tokens.1, s32[2,1024]{1,0:T(2,128)} %bitcast.14, f32[2,1024]{1,0:T(2,128)} %bitcast.15, bf16[1,128]{1,0:T(2,128)(2,1)} %bitcast.16, bf16[1,128]{1,0:T(2,128)(2,1)} %bitcast.17, bf16[448,2048]{1,0:T(8,128)(2,1)} %bitcast.11, bf16[448,2048]{1,0:T(8,128)(2,1)} %bitcast.12, ...), custom_call_target="tpu_custom_call" | custom-call | tf_op jit(solution)/shard_map/experts/pallas_call | solution.py:605
  124.6 1.7 %copy.10 = bf16[1024,128]{1,0:T(8,128)(2,1)} copy(bf16[1024,128]{1,0:T(8,128)(2,1)} %experts.1) | data formatting | bytes 524288
